TPU v7x, 32 devices: a whole 2x2x4 slice. The times are simulated.
32 devices in a mesh: sp: 8 (over z, y), tp: 4 (over x, core).
Axes of the slice: x: 2, y: 2, z: 4, core: 2. Of those that a mesh axis runs over, the one named last changes fastest.
Arguments:
- tokens: bfloat16 [1024, 6, 2048], P(('sp', 'tp')), may hold values from -6 to 6
- norm_gain: float32 [2048], replicated, may hold values from 0.1 to 1.9
- w_query: bfloat16 [3, 2048, 1024], P(None, 'sp', 'tp'), may hold values from -0.125 to 0.125
- w_key: bfloat16 [3, 2048, 1024], P(None, 'sp', 'tp'), may hold values from -0.125 to 0.125
- w_value: bfloat16 [3, 2048, 1024], P(None, 'sp', 'tp'), may hold values from -0.125 to 0.125
- w_out: bfloat16 [1024, 2048], P('tp', 'sp'), may hold values from -0.1875 to 0.1875
Outputs:
- mixed: bfloat16 [1024, 6, 2048], P(('sp', 'tp'))
- log_weight: float32 [1024, 6, 8], P('sp', None, 'tp')
All inputs are finite; a program needn't handle non-finite values.
Results may differ from a plain program's by a relative error of at most 0.015.
Values may be sent and summed in bfloat16 or wider, within the bound.
A program may use at most 128 MiB of HBM per device.

v0:
```python
import math

import jax
import jax.numpy as jnp
from jax import lax
from jax.sharding import PartitionSpec as P

GROUPS = 3
HEADS = 8
STEPS = 24
DILATION_MIDDLE = 4
DILATION_WIDE = 16


epsilon = 1e-06


def from_behind(block, axis, distance):
    devices = range(lax.axis_size(axis))
    route = [(i - distance, i) for i in devices if i - distance in devices]
    return lax.ppermute(block, axis, route)


def on_whole(value, axis, dim, block):
    whole = lax.all_gather(value, axis, axis=dim, tiled=True)
    return block(whole, jnp.int32(0))


def summed_rows(portion, width, axis):
    count = width * lax.axis_size(axis)
    sent = portion(jnp.int32(0), count).astype(jnp.bfloat16)
    return lax.psum_scatter(sent, axis, scatter_dimension=0, tiled=True).astype(jnp.float32)


def rms_normed(values, gain):
    widened = values.astype(jnp.float32)
    scaled = widened * lax.rsqrt(jnp.mean(widened * widened, axis=-1, keepdims=True) + epsilon)
    return (scaled * gain.astype(jnp.float32)).astype(jnp.bfloat16)


def reach_back(pairs, reaches):
    local_rows = pairs.shape[0]
    holding = pairs
    covered = 1
    while covered < max(reaches) + 1:
        arrived = from_behind(holding, "sp", covered)
        holding = jnp.concatenate((arrived, holding), 0)
        covered = covered * 2
    held_rows = holding.shape[0]
    extended = [
        holding[held_rows - (reach + 1) * local_rows :, :, :, group_index]
        for group_index, reach in enumerate(reaches)
    ]
    return extended


def attend_group(queries, extended, reach, dilation):
    local_rows, batch_count, local_heads, head_width = queries.shape
    span_rows = extended.shape[0]
    keys = extended[:, :, 0].reshape(
        span_rows // dilation, dilation, batch_count, local_heads, head_width
    )
    values = extended[:, :, 1].reshape(
        span_rows // dilation, dilation, batch_count, local_heads, head_width
    )
    strided = queries.reshape(
        local_rows // dilation, dilation, batch_count, local_heads, head_width
    )
    scores = jnp.einsum("qrbhe,krbhe->rbhqk", strided, keys, preferred_element_type=jnp.float32)
    scores = scores * (1.0 / math.sqrt(head_width))
    shape_steps = (local_rows // dilation, span_rows // dilation)
    query_step = lax.broadcasted_iota(jnp.int32, shape_steps, 0)
    key_step = lax.broadcasted_iota(jnp.int32, shape_steps, 1)
    lag_steps = query_step + reach * (local_rows // dilation) - key_step
    anchor = (lax.axis_index("sp") - reach) * (local_rows // dilation)
    allowed = (lag_steps >= 0) & (lag_steps <= STEPS) & (key_step + anchor >= 0)
    scores = jnp.where(allowed, scores, jnp.float32(-1e30))
    peak = jnp.max(scores, axis=-1, keepdims=True)
    lifted = jnp.exp(scores - peak)
    totals = jnp.sum(lifted, axis=-1, keepdims=True)
    log_sum = (peak + jnp.log(totals))[..., 0]
    weights = (lifted / totals).astype(jnp.bfloat16)
    mixed = jnp.einsum(
        "rbhqk,krbhe->qrbhe", weights, values, preferred_element_type=jnp.float32
    ).astype(jnp.bfloat16)
    mixed = mixed.reshape(local_rows, batch_count, local_heads, head_width)
    log_rows = jnp.transpose(log_sum, (3, 0, 1, 2)).reshape(local_rows, batch_count, local_heads)
    return (mixed, log_rows)


def shards(tokens, norm_gain, w_query, w_key, w_value, w_out):
    query_full, key_full, value_full, out_full = (
        lax.all_gather(w_query, "sp", axis=1, tiled=True),
        lax.all_gather(w_key, "sp", axis=1, tiled=True),
        lax.all_gather(w_value, "sp", axis=1, tiled=True),
        lax.all_gather(w_out, "sp", axis=1, tiled=True),
    )
    roles = jnp.stack((query_full, key_full, value_full))
    normed = rms_normed(tokens, norm_gain)

    def project(piece, start):
        return jnp.einsum(
            "tbd,rgdc->tbrgc", piece, roles, preferred_element_type=jnp.float32
        ).astype(jnp.bfloat16)

    projected = on_whole(normed, "tp", 0, project)
    local_rows = projected.shape[0]
    batch_count = projected.shape[1]
    local_heads = HEADS // lax.axis_size("tp")
    head_width = projected.shape[-1] // local_heads
    dilations = (1, DILATION_MIDDLE, DILATION_WIDE)
    reaches = tuple((-(-STEPS * dilation // local_rows) for dilation in dilations))
    pairs = projected[:, :, 1:]
    extended = [
        reach_back(pairs[:, :, :, group_index : group_index + 1], (reaches[group_index],))[0]
        for group_index in range(GROUPS)
    ]
    results = []
    for group_index in range(GROUPS):
        queries = projected[:, :, 0, group_index].reshape(
            local_rows, batch_count, local_heads, head_width
        )
        results.append(
            attend_group(
                queries, extended[group_index], reaches[group_index], dilations[group_index]
            )
        )
    stacked_logs = jnp.stack([result[1] for result in results])
    top_log = jnp.max(stacked_logs, axis=0)
    log_weight = top_log + jnp.log(jnp.sum(jnp.exp(stacked_logs - top_log[None]), axis=0))
    shares = jax.nn.softmax(stacked_logs, axis=0)
    outputs = jnp.stack([result[0] for result in results]).astype(jnp.float32)
    combined = jnp.sum(shares[..., None] * outputs, axis=0).astype(jnp.bfloat16)
    combined = combined.reshape(local_rows, batch_count, local_heads * head_width)

    def output_rows(begin, count):
        selected = lax.dynamic_slice_in_dim(combined, begin, count, 0)
        return jnp.einsum("tbc,cd->tbd", selected, out_full, preferred_element_type=jnp.float32)

    mixed = summed_rows(output_rows, local_rows // lax.axis_size("tp"), "tp").astype(jnp.bfloat16)
    return (mixed, log_weight)


def solution(mesh):
    in_specs = (
        P(("sp", "tp"), None, None),
        P(),
        P(None, "sp", "tp"),
        P(None, "sp", "tp"),
        P(None, "sp", "tp"),
        P("tp", "sp"),
    )
    out_specs = (P(("sp", "tp"), None, None), P("sp", None, "tp"))
    return jax.shard_map(shards, mesh=mesh, in_specs=in_specs, out_specs=out_specs, check_vma=False)
```

profile of v0, /device:TPU:17, one launch (start us, length us, event | category | flops | bytes accessed | tf_op | source)
XLA Modules:
  0.0 397.7 jit_solution(10402582273136703270)
XLA Ops:
  8.6 2.3 fusion.11
  14.2 26.6 %all-gather.6.cloned.1.call-done = bf16[128,6,2048]{2,0,1:T(8,128)(2,1)} async-done(((bf16[32,6,2048]{2,0,1:T(8,128)(2,1)}), bf16[128,6,2048]{2,0,1:T(8,128)(2,1)}) %all-gather.6.cloned.1.call-update) | async-done | bytes 3145744 | tf_op jit(solution)/shard_map/all_gather | solution.py:25
  40.9 60.3 %all-gather.8.cloned.1.call-done = bf16[3,2048,256]{2,1,0:T(8,128)(2,1)} async-done(((bf16[3,256,256]{2,1,0:T(8,128)(2,1)}), bf16[3,2048,256]{2,1,0:T(8,128)(2,1)}) %all-gather.8.cloned.1.call-update) | async-done | bytes 3145744 | tf_op jit(solution)/shard_map/all_gather | solution.py:93
  101.2 61.0 %all-gather.10.cloned.1.call-done = bf16[3,2048,256]{2,1,0:T(8,128)(2,1)} async-done(((bf16[3,256,256]{2,1,0:T(8,128)(2,1)}), bf16[3,2048,256]{2,1,0:T(8,128)(2,1)}) %all-gather.10.cloned.1.call-update) | async-done | bytes 3145744 | tf_op jit(solution)/shard_map/all_gather | solution.py:94
  162.2 60.8 %all-gather.12.cloned.1.call-done = bf16[3,2048,256]{2,1,0:T(8,128)(2,1)} async-done(((bf16[3,256,256]{2,1,0:T(8,128)(2,1)}), bf16[3,2048,256]{2,1,0:T(8,128)(2,1)}) %all-gather.12.cloned.1.call-update) | async-done | bytes 3145744 | tf_op jit(solution)/shard_map/all_gather | solution.py:95
  223.0 12.3 %fusion.6 = bf16[128,6,3,3,256]{4,0,3,2,1:T(8,128)(2,1)S(1)} fusion(bf16[1,3,2048,256]{3,2,1,0:T(8,128)(2,1)} %bitcast.109, bf16[1,3,2048,256]{3,2,1,0:T(8,128)(2,1)} %bitcast.108, bf16[1,3,2048,256]{3,2,1,0:T(8,128)(2,1)} %bitcast.107, bf16[128,6,2048]{2,0,1:T(8,128)(2,1)} %all-gather.6.cloned.1.call-done), kind=kOutput, calls=%fused_computation.9 | convolution fusion | flops 7277838336 | bytes 16121856 | tf_op jit(solution)/shard_map/tbd,rgdc->tbrgc/dot_general | solution.py:102
  235.4 2.2 collective-permute-start.1
  238.4 3.8 collective-permute-start.2
  243.2 1.8 reshape_reshape_squeeze.8
  245.0 1.8 reshape_reshape_squeeze.7
  246.9 2.0 collective-permute-start
  249.7 13.8 %collective-permute-done.1 = bf16[128,6,2,1,256]{4,0,3,2,1:T(8,128)(2,1)} collective-permute-done((bf16[128,6,2,1,256]{4,0,3,2,1:T(8,128)(2,1)S(1)}, bf16[128,6,2,1,256]{4,0,3,2,1:T(8,128)(2,1)}, u32[]{:S(2)}, u32[]{:S(2)}) %collective-permute-start.1) | collective-permute-done | bytes 786464 | tf_op jit(solution)/shard_map/ppermute | solution.py:21
  265.7 2.7 reshape_squeeze.14
  272.7 10.8 %collective-permute-done.2 = bf16[128,6,2,1,256]{4,0,3,2,1:T(8,128)(2,1)S(1)} collective-permute-done((bf16[128,6,2,1,256]{4,0,3,2,1:T(8,128)(2,1)S(1)}, bf16[128,6,2,1,256]{4,0,3,2,1:T(8,128)(2,1)S(1)}, u32[]{:S(2)}, u32[]{:S(2)}) %collective-permute-start.2) | collective-permute-done | bytes 786464 | tf_op jit(solution)/shard_map/ppermute | solution.py:21
  284.8 3.5 collective-permute-start.3
  288.3 12.1 %collective-permute-done = bf16[128,6,2,1,256]{4,0,3,2,1:T(8,128)(2,1)} collective-permute-done((bf16[128,6,2,1,256]{4,0,3,2,1:T(8,128)(2,1)S(1)}, bf16[128,6,2,1,256]{4,0,3,2,1:T(8,128)(2,1)}, u32[]{:S(2)}, u32[]{:S(2)}) %collective-permute-start) | collective-permute-done | bytes 786464 | tf_op jit(solution)/shard_map/ppermute | solution.py:21
  302.7 2.7 reshape.133
  313.4 6.6 %collective-permute-done.3 = bf16[256,6,2,1,256]{4,0,3,2,1:T(8,128)(2,1)} collective-permute-done((bf16[256,6,2,1,256]{4,0,3,2,1:T(8,128)(2,1)}, bf16[256,6,2,1,256]{4,0,3,2,1:T(8,128)(2,1)}, u32[]{:S(2)}, u32[]{:S(2)}) %collective-permute-start.3) | collective-permute-done | bytes 1572896 | tf_op jit(solution)/shard_map/ppermute | solution.py:21
  322.9 2.4 reshape_squeeze.15
  325.2 2.1 fusion.68
  329.3 1.9 reshape_squeeze.17
  331.2 2.4 fusion.27
  334.4 3.9 convolution_convert_fusion
  338.9 51.9 %reduce-scatter.2.cloned.1.call-done = bf16[32,6,2048]{2,0,1:T(8,128)(2,1)} async-done(((bf16[128,6,2048]{2,0,1:T(8,128)(2,1)}), bf16[32,6,2048]{2,0,1:T(8,128)(2,1)}) %reduce-scatter.2.cloned.1.call-update) | async-done | bytes 786448 | tf_op jit(solution)/shard_map/reduce_scatter | solution.py:32
  (89 shorter events, 31.5 us)
Async XLA Ops:
  7.2 33.7 %all-gather.6.cloned.1.call-start = ((), (), s32[]{:S(2)}) async-start(), calls=%async_computation.1 | async-start | bytes 3932160 | tf_op jit(solution)/shard_map/all_gather | solution.py:25
  10.9 90.3 %all-gather.8.cloned.1.call-start = ((), (), s32[]{:S(2)}) async-start(), calls=%async_computation.2 | async-start | bytes 3538944 | tf_op jit(solution)/shard_map/all_gather | solution.py:93
  11.6 150.5 %all-gather.10.cloned.1.call-start = ((), (), s32[]{:S(2)}) async-start(), calls=%async_computation.3 | async-start | bytes 3538944 | tf_op jit(solution)/shard_map/all_gather | solution.py:94
  12.4 210.6 %all-gather.12.cloned.1.call-start = ((), (), s32[]{:S(2)}) async-start(), calls=%async_computation.4 | async-start | bytes 3538944 | tf_op jit(solution)/shard_map/all_gather | solution.py:95
  12.9 321.4 %all-gather.14.cloned.1.call-start = ((), (), s32[]{:S(2)}) async-start(), calls=%async_computation.5 | async-start | bytes 1179648 | tf_op jit(solution)/shard_map/all_gather | solution.py:96
  13.5 377.3 %reduce-scatter.2.cloned.1.call-start = ((), (), s32[]{:S(2)}) async-start(), calls=%async_computation.6 | async-start | bytes 3932160 | tf_op jit(solution)/shard_map/reduce_scatter | solution.py:32
  235.4 28.0 %collective-permute-start.1 = (bf16[128,6,2,1,256]{4,0,3,2,1:T(8,128)(2,1)S(1)}, bf16[128,6,2,1,256]{4,0,3,2,1:T(8,128)(2,1)}, u32[]{:S(2)}, u32[]{:S(2)}) collective-permute-start(bf16[128,6,2,1,256]{4,0,3,2,1:T(8,128)(2,1)S(1)} %get-tuple-element.9), channel_id=1, source_target_pairs={{0,4},{4,8},{8,12},{12,16},{16,20},{20,24},{24,28},{1,5},{5,9},{9,... | collective-permute-start | bytes 2359304 | tf_op jit(solution)/shard_map/ppermute | solution.py:21
  238.4 45.1 %collective-permute-start.2 = (bf16[128,6,2,1,256]{4,0,3,2,1:T(8,128)(2,1)S(1)}, bf16[128,6,2,1,256]{4,0,3,2,1:T(8,128)(2,1)S(1)}, u32[]{:S(2)}, u32[]{:S(2)}) collective-permute-start(bf16[128,6,2,1,256]{4,0,3,2,1:T(8,128)(2,1)S(1)} %get-tuple-element.8), channel_id=1, source_target_pairs={{0,4},{4,8},{8,12},{12,16},{16,20},{20,24},{24,28},{1,5},{5,9},{9,... | collective-permute-start | bytes 2359304 | tf_op jit(solution)/shard_map/ppermute | solution.py:21
  246.9 53.6 %collective-permute-start = (bf16[128,6,2,1,256]{4,0,3,2,1:T(8,128)(2,1)S(1)}, bf16[128,6,2,1,256]{4,0,3,2,1:T(8,128)(2,1)}, u32[]{:S(2)}, u32[]{:S(2)}) collective-permute-start(bf16[128,6,2,1,256]{4,0,3,2,1:T(8,128)(2,1)S(1)} %get-tuple-element.7), channel_id=1, source_target_pairs={{0,4},{4,8},{8,12},{12,16},{16,20},{20,24},{24,28},{1,5},{5,9},{9,... | collective-permute-start | bytes 2359304 | tf_op jit(solution)/shard_map/ppermute | solution.py:21
  264.7 3.7 copy-start.7
  270.2 0.9 copy-start.4
  270.2 0.9 copy-start.9
  284.8 35.2 %collective-permute-start.3 = (bf16[256,6,2,1,256]{4,0,3,2,1:T(8,128)(2,1)}, bf16[256,6,2,1,256]{4,0,3,2,1:T(8,128)(2,1)}, u32[]{:S(2)}, u32[]{:S(2)}) collective-permute-start(bf16[256,6,2,1,256]{4,0,3,2,1:T(8,128)(2,1)} %pad_maximum_fusion), channel_id=1, source_target_pairs={{0,8},{4,12},{8,16},{12,20},{16,24},{20,28},{1,9},{5,13},{9,17},{1... | collective-permute-start | bytes 4718600 | tf_op jit(solution)/shard_map/ppermute | solution.py:21
  302.7 4.1 %copy-start.10 = (f32[4,6,2,32]{3,2,1,0:T(2,128)S(1)}, f32[4,6,2,32]{3,2,1,0:T(2,128)}, u32[]{:S(2)}) copy-start(f32[4,6,2,32]{3,2,1,0:T(2,128)} %copy-done.9) | copy-start | bytes 18436
  306.8 2.4 copy-start.6
  309.2 2.7 copy-start.5
  327.4 0.9 copy-start
  327.4 1.5 copy-start.2
  328.9 2.3 copy-start.1
  329.0 2.2 copy-start.3
  331.2 2.8 copy-start.12
  331.2 2.8 copy-start.11
  331.2 2.8 copy-start.13
  331.2 2.9 copy-start.8
Sparse Core Ops, SparseCore 0:
  11.0 29.8 all-gather.5
  43.1 58.0 all-gather.7
  103.4 58.7 all-gather.9
  164.2 58.7 all-gather.11
  224.9 42.8 all-gather.13
  338.4 52.3 reduce-scatter.1
where the time goes:
time: 400 us; the launch traced here: 398 us
  waiting for transfers between devices  306 us (76%)
  matrix products  27.3 us (7%)
  local copies, waits for them, and re-layouts  24.1 us (6%)
  between operations  14.5 us (4%)
  other arithmetic  13.6 us (3%)
  starting transfers between devices  11.7 us (3%)
    all_gather x1, waiting for transfers between devices, shards(): lax.all_gather(w_key, 'sp', axis=1, tiled=True)  61 us
    all_gather x1, waiting for transfers between devices, shards(): lax.all_gather(w_value, 'sp', axis=1, tiled=True)  60.8 us
    all_gather x1, waiting for transfers between devices, shards(): lax.all_gather(w_query, 'sp', axis=1, tiled=True)  60.3 us
    reduce_scatter x1, waiting for transfers between devices, summed_rows(): lax.psum_scatter(sent, axis, scatter_dimension=0, tiled=True)  51.9 us
    ppermute x4, waiting for transfers between devices, from_behind(): return lax.ppermute(block, axis, route)  43.2 us
    all_gather x1, waiting for transfers between devices, on_whole(): whole = lax.all_gather(value, axis, axis=dim, tiled=True)  26.6 us
    dot_general x1, matrix products, project(): jnp.einsum('tbd,rgdc->tbrgc', piece, roles, preferred_element_type=jnp.fl...  12.3 us
    ppermute x4, starting transfers between devices, from_behind(): return lax.ppermute(block, axis, route)  11.5 us
  transfers between devices with their start and end apart: 10, of which 9 were waited for; matrix products, arithmetic and copies ran while one was open for 14% of the time, Pallas kernels for 0%

commit v1 on v0

v1 whole, which is shorter than its diff:
```python
import functools
import math

import jax
import jax.numpy as jnp
from jax import lax
from jax.experimental import pallas as pl
from jax.experimental.pallas import tpu as pltpu
from jax.sharding import PartitionSpec as P

GROUPS = 3
HEADS = 8
STEPS = 24
DILATION_MIDDLE = 4
DILATION_WIDE = 16
DILATIONS = (1, DILATION_MIDDLE, DILATION_WIDE)
MESH = pl.DeviceIdType.MESH
PAIR = 2

epsilon = 1e-06


def rms_normed(values, gain):
    widened = values.astype(jnp.float32)
    scaled = widened * lax.rsqrt(jnp.mean(widened * widened, axis=-1, keepdims=True) + epsilon)
    return (scaled * gain.astype(jnp.float32)).astype(jnp.bfloat16)


def remote(src, dst, send, recv, where):
    return pltpu.make_async_remote_copy(
        src_ref=src, dst_ref=dst, send_sem=send, recv_sem=recv, device_id=where, device_id_type=MESH
    )


def gather_kernel(
    n, m, x_ref, q_ref, k_ref, v_ref, o_ref, xf, qf, kf, vf, of,
    local, up_s, up_r, dn_s, dn_r, y_s, y_r, x_s, x_r, o_s, o_r,
):
    s, t = lax.axis_index("sp"), lax.axis_index("tp")
    nz = n // PAIR
    z, y = lax.div(s, PAIR), lax.rem(s, PAIR)
    partner = {"sp": s + 1 - 2 * y}
    above, below = {"sp": s + PAIR}, {"sp": s - PAIR}
    has_above, has_below = z + 1 < nz, z > 0
    peers = [lax.rem(t + i, m) for i in range(1, m)]
    depth, wide, tall = q_ref.shape[1], o_ref.shape[1], o_ref.shape[0]
    rows = x_ref.shape[1]

    barrier = pltpu.get_barrier_semaphore()
    pl.semaphore_signal(barrier, inc=1, device_id=partner, device_id_type=MESH)
    for peer in peers:
        pl.semaphore_signal(barrier, inc=1, device_id={"tp": peer}, device_id_type=MESH)

    @pl.when(has_above)
    def _():
        pl.semaphore_signal(barrier, inc=1, device_id=above, device_id_type=MESH)

    @pl.when(has_below)
    def _():
        pl.semaphore_signal(barrier, inc=1, device_id=below, device_id_type=MESH)

    pl.semaphore_wait(barrier, m + has_above.astype(jnp.int32) + has_below.astype(jnp.int32))

    fulls = (qf, kf, vf)
    owns = (q_ref, k_ref, v_ref)
    tall_rows = pl.ds(pl.multiple_of(t * tall, tall), tall)

    def weight_block(p, zk, side=None):
        index = zk * PAIR + (y if side is None else side)
        return fulls[p].at[:, pl.ds(pl.multiple_of(index * depth, depth), depth), :]

    def out_pair(zk, owner=None):
        at = tall_rows if owner is None else pl.ds(pl.multiple_of(owner * tall, tall), tall)
        if len(of.shape) == 3:
            return of.at[pl.ds(zk * PAIR, PAIR), at, :]
        return of.at[at, pl.ds(pl.multiple_of(zk * PAIR * wide, PAIR * wide), PAIR * wide)]

    def out_own(index):
        if len(of.shape) == 3:
            return of.at[index, tall_rows, :]
        return of.at[tall_rows, pl.ds(pl.multiple_of(index * wide, wide), wide)]

    def x_rows(owner):
        return xf.at[:, pl.ds(pl.multiple_of(owner * rows, rows), rows), :]

    o_local = pltpu.make_async_copy(o_ref, out_own(s), local.at[3])
    o_local.start()
    o_swap = remote(o_ref, out_own(s), y_s.at[0, 0, 3], y_r.at[0, 0, 3], partner)
    o_swap.start()
    token_sends = []
    for i, peer in enumerate(peers):
        c = remote(x_ref, x_rows(t), x_s.at[i], x_r.at[i], {"tp": peer})
        c.start()
        token_sends.append(c)
    locals_ = [pltpu.make_async_copy(x_ref, x_rows(t), local.at[4])]
    for p in range(3):
        locals_.append(pltpu.make_async_copy(owns[p], weight_block(p, z), local.at[p]))
    for c in locals_:
        c.start()
    o_local.wait()
    o_swap.wait()

    def line(up, k, p):
        zk = z - k if up else z + k
        where = above if up else below
        sems = (up_s, up_r) if up else (dn_s, dn_r)
        if p == 3:
            src = out_pair(zk)
            dst = src
        else:
            dst = weight_block(p, zk)
            src = owns[p] if k == 0 else dst
        return remote(src, dst, sems[0].at[k, p], sems[1].at[k, p], where)

    def sideways(up, k, p):
        zk = z - k if up else z + k
        dst = weight_block(p, zk)
        src = owns[p] if k == 0 else dst
        a = 0 if up else 1
        return remote(src, dst, y_s.at[a, k, p], y_r.at[a, k, p], partner)

    def spread(up, k, i):
        zk = z - k if up else z + k
        a = 0 if up else 1
        return remote(out_pair(zk), out_pair(zk), o_s.at[a, k, i], o_r.at[a, k, i], {"tp": peers[i]})

    def arrival(up, k, p):
        zk = z - k if up else z + k
        sems = (up_s, up_r) if up else (dn_s, dn_r)
        dst = out_pair(zk) if p == 3 else weight_block(p, zk)
        return remote(dst, dst, sems[0].at[k - 1, p], sems[1].at[k - 1, p], below if up else above)

    def present(up, k):
        return z - k >= 0 if up else z + k < nz

    def onward(up, k):
        return jnp.logical_and(present(up, k), has_above if up else has_below)

    for k in range(nz):
        for p in (3, 0, 1, 2):
            for up in (True, False):
                def have(up=up, k=k, p=p):
                    if k > 0:
                        arrival(up, k, p).wait_recv()
                    if k < nz - 1:
                        @pl.when(has_above if up else has_below)
                        def _():
                            line(up, k, p).start()
                    if k > 0 or up:
                        if p == 3:
                            for i in range(m - 1):
                                spread(up, k, i).start()
                        else:
                            sideways(up, k, p).start()
                if k == 0:
                    have()
                else:
                    pl.when(present(up, k))(have)

    for c in locals_:
        c.wait()
    for i in range(m - 1):
        token_sends[i].wait_send()
        sender = lax.rem(t + m - 1 - i, m)
        remote(x_ref, x_rows(sender), x_s.at[i], x_r.at[i], {"tp": sender}).wait_recv()
    for k in range(nz):
        for up in (True, False):
            if k < nz - 1:
                @pl.when(onward(up, k))
                def _(up=up, k=k):
                    for p in range(4):
                        line(up, k, p).wait_send()
            if k > 0 or up:
                @pl.when(present(up, k))
                def _(up=up, k=k):
                    zk = z - k if up else z + k
                    a = 0 if up else 1
                    for p in range(3):
                        sideways(up, k, p).wait_send()
                        came = weight_block(p, zk, 1 - y)
                        remote(came, came, y_s.at[a, k, p], y_r.at[a, k, p], partner).wait_recv()
                    for i in range(m - 1):
                        spread(up, k, i).wait_send()
                        sender = lax.rem(t + m - 1 - i, m)
                        came = out_pair(zk, sender)
                        remote(came, came, o_s.at[a, k, i], o_r.at[a, k, i], {"tp": sender}).wait_recv()


def gather_all(x, wq, wk, wv, wo, n, m):
    nz = n // PAIR
    groups, depth, cols = wq.shape
    full_w = jax.ShapeDtypeStruct((groups, depth * n, cols), wq.dtype)
    tall, wide = wo.shape
    blocked = wide % 128 != 0
    out_shape = (n, tall * m, wide) if blocked else (tall * m, wide * n)
    dma = pltpu.SemaphoreType.DMA
    *gathered, out_full = pl.pallas_call(
        functools.partial(gather_kernel, n, m),
        out_shape=(
            jax.ShapeDtypeStruct((x.shape[0], x.shape[1] * m, x.shape[2]), x.dtype),
            full_w, full_w, full_w,
            jax.ShapeDtypeStruct(out_shape, wo.dtype),
        ),
        in_specs=[pl.BlockSpec(memory_space=pltpu.VMEM)] * 5,
        out_specs=(pl.BlockSpec(memory_space=pl.ANY),) * 5,
        scratch_shapes=[
            dma((5,)), dma((nz, 4)), dma((nz, 4)), dma((nz, 4)), dma((nz, 4)),
            dma((2, nz, 4)), dma((2, nz, 4)), dma((m - 1,)), dma((m - 1,)),
            dma((2, nz, m - 1)), dma((2, nz, m - 1)),
        ],
        compiler_params=pltpu.CompilerParams(collective_id=0, has_side_effects=True),
    )(x, wq, wk, wv, wo)
    if blocked:
        out_full = jnp.transpose(out_full, (1, 0, 2)).reshape(tall * m, wide * n)
    return (*gathered, out_full)


def halo_parts(local_rows):
    parts = []
    for g, dilation in enumerate(DILATIONS):
        reach = STEPS * dilation
        for hop in range(1, -(-reach // local_rows) + 1):
            count = min(local_rows, reach - (hop - 1) * local_rows)
            parts.append((g, hop, count, reach - (hop - 1) * local_rows - count))
    return parts


def halo_kernel(n, k_ref, v_ref, *refs):
    halos, (send, recv) = refs[: 2 * GROUPS], refs[2 * GROUPS :]
    s = lax.axis_index("sp")
    local_rows = k_ref.shape[2]
    parts = halo_parts(local_rows)
    farthest = max(hop for _, hop, _, _ in parts)
    barrier = pltpu.get_barrier_semaphore()
    count = jnp.int32(0)
    for hop in range(1, farthest + 1):
        ahead, behind = s + hop < n, s - hop >= 0

        @pl.when(ahead)
        def _():
            pl.semaphore_signal(barrier, inc=1, device_id={"sp": s + hop}, device_id_type=MESH)

        @pl.when(behind)
        def _():
            pl.semaphore_signal(barrier, inc=1, device_id={"sp": s - hop}, device_id_type=MESH)

        count = count + ahead.astype(jnp.int32) + behind.astype(jnp.int32)
    pl.semaphore_wait(barrier, count)

    def copy(index, role):
        g, hop, rows, at = parts[index]
        src = (k_ref, v_ref)[role].at[g, :, pl.ds(local_rows - rows, rows), :]
        dst = halos[role * GROUPS + g].at[:, pl.ds(at, rows), :]
        return remote(src, dst, send.at[index, role], recv.at[index, role], {"sp": s + hop})

    order = sorted(range(len(parts)), key=lambda i: -parts[i][1])
    for index in order:
        @pl.when(s + parts[index][1] < n)
        def _():
            for role in range(2):
                copy(index, role).start()
    for index in order:
        @pl.when(s + parts[index][1] < n)
        def _():
            for role in range(2):
                copy(index, role).wait_send()

        @pl.when(s - parts[index][1] >= 0)
        def _():
            for role in range(2):
                copy(index, role).wait_recv()


def exchange_halos(keys, values, n):
    _, batch, rows, cols = keys.shape
    shapes = tuple(
        jax.ShapeDtypeStruct((batch, STEPS * d, cols), keys.dtype) for d in DILATIONS
    )
    parts = len(halo_parts(rows))
    return pl.pallas_call(
        functools.partial(halo_kernel, n),
        out_shape=shapes + shapes,
        in_specs=[pl.BlockSpec(memory_space=pl.ANY)] * 2,
        out_specs=(pl.BlockSpec(memory_space=pl.ANY),) * (2 * GROUPS),
        scratch_shapes=[pltpu.SemaphoreType.DMA((parts, 2)), pltpu.SemaphoreType.DMA((parts, 2))],
        compiler_params=pltpu.CompilerParams(collective_id=1, has_side_effects=True),
    )(keys, values)


def attend_kernel(place, q_ref, k_ref, v_ref, *refs):
    halos, (out_ref, log_ref) = refs[: 2 * GROUPS], refs[2 * GROUPS :]
    rows, cols = q_ref.shape[2], q_ref.shape[3]
    heads = log_ref.shape[1]
    width = cols // heads
    start = place[0] * rows
    for h in range(heads):
        lanes = slice(h * width, (h + 1) * width)
        logs, outs = [], []
        for g, dilation in enumerate(DILATIONS):
            reach = STEPS * dilation
            query = q_ref[g, 0, :, lanes]

            def scored(key, first, count):
                score = lax.dot_general(query, key, (((1,), (1,)), ((), ())), preferred_element_type=jnp.float32)
                score = score * (1.0 / math.sqrt(width))
                lag = lax.broadcasted_iota(jnp.int32, (rows, count), 0) - lax.broadcasted_iota(jnp.int32, (rows, count), 1) - first
                at = lax.broadcasted_iota(jnp.int32, (rows, count), 1) + (first + start)
                allowed = (lag >= 0) & (lag <= reach) & ((lag & (dilation - 1)) == 0) & (at >= 0)
                return jnp.where(allowed, score, jnp.float32(-1e30))

            near = scored(k_ref[g, 0, :, lanes], 0, rows)
            far = scored(halos[g][0, :, lanes], -reach, reach)
            peak = jnp.maximum(jnp.max(near, axis=1, keepdims=True), jnp.max(far, axis=1, keepdims=True))
            near, far = jnp.exp(near - peak), jnp.exp(far - peak)
            total = jnp.sum(near, axis=1, keepdims=True) + jnp.sum(far, axis=1, keepdims=True)
            logs.append(peak + jnp.log(total))
            known = lax.broadcasted_iota(jnp.int32, (reach, width), 0) + (start - reach) >= 0
            old = halos[GROUPS + g][0, :, lanes]
            old = jnp.where(known, old.astype(jnp.float32), 0.0).astype(jnp.bfloat16)
            mixed = jnp.dot((near / total).astype(jnp.bfloat16), v_ref[g, 0, :, lanes], preferred_element_type=jnp.float32)
            mixed = mixed + jnp.dot((far / total).astype(jnp.bfloat16), old, preferred_element_type=jnp.float32)
            outs.append(mixed.astype(jnp.bfloat16).astype(jnp.float32))
        top = functools.reduce(jnp.maximum, logs)
        shares = [jnp.exp(log - top) for log in logs]
        whole = sum(shares)
        log_ref[0, h] = top + jnp.log(whole)
        combined = sum((share / whole) * out for share, out in zip(shares, outs))
        out_ref[0, :, lanes] = combined.astype(jnp.bfloat16)


def attend(place, q, k, v, halos, heads):
    groups, batch, rows, cols = q.shape
    main = pl.BlockSpec((groups, 1, rows, cols), lambda b: (0, b, 0, 0))
    halo_specs = [pl.BlockSpec((1, h.shape[1], cols), lambda b: (b, 0, 0)) for h in halos]
    return pl.pallas_call(
        attend_kernel,
        grid=(batch,),
        out_shape=(
            jax.ShapeDtypeStruct((batch, rows, cols), jnp.bfloat16),
            jax.ShapeDtypeStruct((batch, heads, rows, 1), jnp.float32),
        ),
        in_specs=[pl.BlockSpec(memory_space=pltpu.SMEM), main, main, main] + halo_specs,
        out_specs=(
            pl.BlockSpec((1, rows, cols), lambda b: (b, 0, 0)),
            pl.BlockSpec((1, heads, rows, 1), lambda b: (b, 0, 0, 0)),
        ),
    )(place, q, k, v, *halos)


def swap_kernel(m, c_ref, out, local, send, recv):
    t = lax.axis_index("tp")
    rows, cols = out.shape[1], c_ref.shape[2]
    peers = [lax.rem(t + i, m) for i in range(1, m)]
    barrier = pltpu.get_barrier_semaphore()
    for peer in peers:
        pl.semaphore_signal(barrier, inc=1, device_id={"tp": peer}, device_id_type=MESH)
    pl.semaphore_wait(barrier, m - 1)

    def piece(owner):
        return c_ref.at[:, pl.ds(pl.multiple_of(owner * rows, rows), rows), :]

    def place(owner):
        return out.at[:, :, pl.ds(pl.multiple_of(owner * cols, cols), cols)]

    copies = [remote(piece(p), place(t), send.at[i], recv.at[i], {"tp": p}) for i, p in enumerate(peers)]
    for c in copies:
        c.start()
    own = pltpu.make_async_copy(piece(t), place(t), local)
    own.start()
    own.wait()
    for i, c in enumerate(copies):
        c.wait_send()
        sender = lax.rem(t + m - 1 - i, m)
        remote(piece(sender), place(sender), send.at[i], recv.at[i], {"tp": sender}).wait_recv()


def swap_heads(combined, m):
    batch, rows, cols = combined.shape
    dma = pltpu.SemaphoreType.DMA
    return pl.pallas_call(
        functools.partial(swap_kernel, m),
        out_shape=jax.ShapeDtypeStruct((batch, rows // m, cols * m), combined.dtype),
        in_specs=[pl.BlockSpec(memory_space=pltpu.VMEM)],
        out_specs=pl.BlockSpec(memory_space=pltpu.VMEM),
        scratch_shapes=[dma, dma((m - 1,)), dma((m - 1,))],
        compiler_params=pltpu.CompilerParams(collective_id=2, has_side_effects=True),
    )(combined)


def shards(tokens, norm_gain, w_query, w_key, w_value, w_out):
    n, m = lax.axis_size("sp"), lax.axis_size("tp")
    normed = rms_normed(jnp.transpose(tokens, (1, 0, 2)), norm_gain)
    rows, query_full, key_full, value_full, out_full = gather_all(normed, w_query, w_key, w_value, w_out, n, m)

    def project(weight):
        return jnp.einsum("btd,gdc->gbtc", rows, weight, preferred_element_type=jnp.float32).astype(jnp.bfloat16)

    keys, values, queries = project(key_full), project(value_full), project(query_full)
    halos = exchange_halos(keys, values, n)
    place = lax.axis_index("sp").astype(jnp.int32).reshape(1)
    combined, logs = attend(place, queries, keys, values, halos, HEADS // m)
    log_weight = jnp.transpose(logs[..., 0], (2, 0, 1))
    swapped = swap_heads(combined, m)
    mixed = jnp.einsum("btc,cd->btd", swapped, out_full, preferred_element_type=jnp.float32).astype(jnp.bfloat16)
    return (jnp.transpose(mixed, (1, 0, 2)), log_weight)


def solution(mesh):
    in_specs = (
        P(("sp", "tp"), None, None),
        P(),
        P(None, "sp", "tp"),
        P(None, "sp", "tp"),
        P(None, "sp", "tp"),
        P("tp", "sp"),
    )
    out_specs = (P(("sp", "tp"), None, None), P("sp", None, "tp"))
    return jax.shard_map(shards, mesh=mesh, in_specs=in_specs, out_specs=out_specs, check_vma=False)
```

time: 400 us -> 250 us (0.62)
  waiting for transfers between devices: 306 us -> 0 us
  Pallas kernels: 0 us -> 225 us
  local copies, waits for them, and re-layouts: 24.1 us -> 0.01 us
  between operations: 14.5 us -> 0.68 us
  starting transfers between devices: 11.7 us -> 0 us
  other arithmetic: 13.6 us -> 4.53 us
  matrix products: 27.3 us -> 20.2 us
    pallas_call x0 -> x4, Pallas kernels: none -> 225 us  [the longest x1 111 us: gather_all(): pl.pallas_call(functools.partial(gather_kernel, n, m), out_shape=(jax.Sha...]
    all_gather x5 -> x0, waiting for transfers between devices: 209 us -> none  [the longest x1 61 us: shards(): lax.all_gather(w_key, 'sp', axis=1, tiled=True)]
    reduce_scatter x1 -> x0, waiting for transfers between devices: 51.9 us -> none  [summed_rows(): lax.psum_scatter(sent, axis, scatter_dimension=0, tiled=True)]
    ppermute x4 -> x0, waiting for transfers between devices: 43.2 us -> none  [from_behind(): return lax.ppermute(block, axis, route)]
    another operation x12 -> x0, local copies, waits for them, and re-layouts: 16 us -> none  [the longest x2 5.07 us: attend_group(): extended[:, :, 0]]
    ppermute x4 -> x0, starting transfers between devices: 11.5 us -> none  [from_behind(): return lax.ppermute(block, axis, route)]
    dot_general x8 -> x4, matrix products: 27.3 us -> 20.2 us  [the longest x3 15.9 us: project(): jnp.einsum('btd,gdc->gbtc', rows, weight, preferred_element_type=jnp.floa...]
    slice x5 -> x0, local copies, waits for them, and re-layouts: 4.51 us -> none  [the longest x3 3.4 us: attend_group(): extended[:, :, 0]]
  transfers between devices with their start and end apart: 10 -> 0, of which waited for: 9 -> 0; matrix products, arithmetic and copies ran while one was open for 14% -> 0% of each run, Pallas kernels for 0% -> 0%
where the time goes in v1:
time: 250 us
  Pallas kernels  225 us (90%)
  matrix products  20.2 us (8%)
  other arithmetic  4.53 us (2%)
    pallas_call x1, Pallas kernels, gather_all(): pl.pallas_call(functools.partial(gather_kernel, n, m), out_shape=(jax.Sha...  111 us
    pallas_call x1, Pallas kernels, exchange_halos(): pl.pallas_call(functools.partial(halo_kernel, n), out_shape=shapes + shap...  87.8 us
    pallas_call x1, Pallas kernels, attend(): pl.pallas_call(attend_kernel, grid=(batch,), out_shape=(jax.ShapeDtypeStr...  16.4 us
    dot_general x3, matrix products, project(): jnp.einsum('btd,gdc->gbtc', rows, weight, preferred_element_type=jnp.floa...  15.9 us
    pallas_call x1, Pallas kernels, swap_heads(): pl.pallas_call(functools.partial(swap_kernel, m), out_shape=jax.ShapeDtyp...  9.18 us

profile of v1, /device:TPU:17, one launch (start us, length us, event | category | flops | bytes accessed | tf_op | source)
XLA Modules:
  0.0 249.9 jit_solution(10700461403019552229)
XLA Ops:
  0.6 1.4 fusion.17
  2.0 2.3 fusion.19.x_ref
  4.3 111.1 %shard_map.77 = (bf16[6,128,2048]{2,1,0:T(8,128)(2,1)}, bf16[3,2048,256]{2,1,0:T(8,128)(2,1)}, bf16[3,2048,256]{2,1,0:T(8,128)(2,1)}, bf16[3,2048,256]{2,1,0:T(8,128)(2,1)}, bf16[1024,2048]{1,0:T(8,128)(2,1)}) custom-call(bf16[6,32,2048]{2,1,0:T(8,128)(2,1)} %fusion.19.x_ref, bf16[3,256,256]{2,1,0:T(8,128)(2,1)} %q_ref.1, bf16[3,256,256]{2,1,0:T(8,128)(2,1)} %k_ref.1, ...), custom_call_target="tpu_custom_call" | custom-call | tf_op jit(solution)/shard_map/pallas_call | solution.py:197
  115.4 0.0 copy-start.1
  115.4 0.0 copy-start.2
  115.4 6.6 %fusion.35.v_ref = bf16[3,6,128,256]{3,2,1,0:T(8,128)(2,1)} fusion(bf16[6,128,2048]{2,1,0:T(8,128)(2,1)} %get-tuple-element.16, bf16[3,2048,256]{2,1,0:T(8,128)(2,1)} %get-tuple-element.18), kind=kOutput, calls=%fused_computation.21 | convolution fusion | flops 2416508928 | bytes 7471104 | tf_op jit(solution)/shard_map/btd,gdc->gbtc/dot_general | solution.py:396
  122.1 0.0 copy-done.1
  122.1 0.0 copy-done.2
  122.1 3.7 %fusion.40.k_ref = bf16[3,6,128,256]{3,2,1,0:T(8,128)(2,1)} fusion(bf16[6,128,2048]{2,1,0:T(8,128)(2,1)S(1)} %copy-done.1, bf16[3,2048,256]{2,1,0:T(8,128)(2,1)S(1)} %copy-done.2), kind=kOutput, calls=%fused_computation.22 | convolution fusion | flops 2416508928 | bytes 7471104 | tf_op jit(solution)/shard_map/btd,gdc->gbtc/dot_general | solution.py:396
  125.8 87.8 %shard_map.78 = (bf16[6,24,256]{2,1,0:T(8,128)(2,1)}, bf16[6,96,256]{2,1,0:T(8,128)(2,1)}, bf16[6,384,256]{2,1,0:T(8,128)(2,1)}, bf16[6,24,256]{2,1,0:T(8,128)(2...) custom-call(bf16[3,6,128,256]{3,2,1,0:T(8,128)(2,1)} %fusion.40.k_ref, bf16[3,6,128,256]{3,2,1,0:T(8,128)(2,1)} %fusion.35.v_ref), custom_call_target="tpu_custom_call" | custom-call | tf_op jit(solution)/shard_map/pallas_call | solution.py:280
  213.6 5.6 %fusion.45.q_ref = bf16[3,6,128,256]{3,2,1,0:T(8,128)(2,1)} fusion(bf16[6,128,2048]{2,1,0:T(8,128)(2,1)S(1)} %copy-done.1, bf16[3,2048,256]{2,1,0:T(8,128)(2,1)} %get-tuple-element.15), kind=kOutput, calls=%fused_computation.23 | convolution fusion | flops 2416508928 | bytes 7471104 | tf_op jit(solution)/shard_map/btd,gdc->gbtc/dot_general | solution.py:396
  219.2 16.4 %shard_map.79 = (bf16[6,128,256]{2,1,0:T(8,128)(2,1)}, f32[6,2,128,1]{3,2,1,0:T(8,128)}) custom-call(s32[1]{0:T(128)} %bitcast.place, bf16[3,6,128,256]{3,2,1,0:T(8,128)(2,1)} %fusion.45.q_ref, bf16[3,6,128,256]{3,2,1,0:T(8,128)(2,1)} %fusion.40.k_ref, bf16[3,6,128,256]{3,2,1,0:T(8,128)(2,1)} %fusion.35.v_ref, ...), custom_call_target="tpu_custom_call" | custom-call | tf_op jit(solution)/shard_map/pallas_call | solution.py:335
  235.6 9.2 %shard_map.80 = bf16[6,32,1024]{2,1,0:T(8,128)(2,1)} custom-call(bf16[6,128,256]{2,1,0:T(8,128)(2,1)} %get-tuple-element.25.c_ref), custom_call_target="tpu_custom_call" | custom-call | tf_op jit(solution)/shard_map/pallas_call | solution.py:380
  244.8 0.0 copy-start
  244.8 4.2 %fusion.14 = bf16[32,6,2048]{2,0,1:T(8,128)(2,1)} fusion(bf16[6,32,1024]{2,1,0:T(8,128)(2,1)} %shard_map.80, bf16[1024,2048]{1,0:T(8,128)(2,1)} %get-tuple-element.26), kind=kOutput, calls=%fused_computation.12 | convolution fusion | flops 805699584 | bytes 5373952 | tf_op jit(solution)/shard_map/btc,cd->btd/dot_general | solution.py:404
  249.0 0.0 copy-done
  249.0 0.9 reduce
  (1 shorter events, 0.0 us)
Async XLA Ops:
  115.4 6.6 %copy-start.1 = (bf16[6,128,2048]{2,1,0:T(8,128)(2,1)S(1)}, bf16[6,128,2048]{2,1,0:T(8,128)(2,1)}, u32[]{:S(2)}) copy-start(bf16[6,128,2048]{2,1,0:T(8,128)(2,1)} %get-tuple-element.16) | copy-start | bytes 9437188
  115.4 6.6 %copy-start.2 = (bf16[3,2048,256]{2,1,0:T(8,128)(2,1)S(1)}, bf16[3,2048,256]{2,1,0:T(8,128)(2,1)}, u32[]{:S(2)}) copy-start(bf16[3,2048,256]{2,1,0:T(8,128)(2,1)} %get-tuple-element.17) | copy-start | bytes 9437188
  244.8 4.3 %copy-start = (f32[6,2,128,1]{3,2,1,0:T(8,128)S(1)}, f32[6,2,128,1]{3,2,1,0:T(8,128)}, u32[]{:S(2)}) copy-start(f32[6,2,128,1]{3,2,1,0:T(8,128)} %get-tuple-element.27) | copy-start | bytes 18436

commit v2 on v1

--- a/solution.py
+++ b/solution.py
@@ -271,7 +271,164 @@
                 copy(index, role).wait_recv()
 
 
+def relay_kernel(n, k_ref, v_ref, *refs):
+    halos, staged, (send, recv) = refs[: 2 * GROUPS], refs[2 * GROUPS : 2 * GROUPS + 4], refs[2 * GROUPS + 4 :]
+    s = lax.axis_index("sp")
+    nz = n // PAIR
+    z, y = lax.div(s, PAIR), lax.rem(s, PAIR)
+    partner, above, below = {"sp": s + 1 - 2 * y}, {"sp": s + PAIR}, {"sp": s - PAIR}
+    up, down, down2 = z + 1 < nz, z > 0, z > 1
+    local_rows = k_ref.shape[2]
+    owns = (k_ref, v_ref)
+    wide = GROUPS - 1
+    barrier = pltpu.get_barrier_semaphore()
+    pl.semaphore_signal(barrier, inc=1, device_id=partner, device_id_type=MESH)
+
+    @pl.when(up)
+    def _():
+        pl.semaphore_signal(barrier, inc=1, device_id=above, device_id_type=MESH)
+
+    @pl.when(down)
+    def _():
+        pl.semaphore_signal(barrier, inc=1, device_id=below, device_id_type=MESH)
+
+    pl.semaphore_wait(barrier, 1 + up.astype(jnp.int32) + down.astype(jnp.int32))
+
+    def slot(hop, r):
+        return halos[r * GROUPS + wide].at[:, pl.ds((3 - hop) * local_rows, local_rows), :]
+
+    def own(r):
+        return owns[r].at[wide]
+
+    def tail(g, r):
+        rows = halos[r * GROUPS + g].shape[1]
+        return owns[r].at[g, :, pl.ds(local_rows - rows, rows), :]
+
+    def move(src, dst, at, r, where, sent=None):
+        return remote(src, dst, send.at[at if sent is None else sent, r], recv.at[at, r], where)
+
+    def landed(hop, r):
+        move(slot(hop, r), slot(hop, r), hop, r, partner).wait_recv()
+
+    both = (0, 1)
+
+    def small(r, g, src=None):
+        return move(tail(g, r) if src is None else src, halos[r * GROUPS + g], 4 + g, r, partner)
+
+    def lift(r, g):
+        return move(tail(g, r), staged[r * 2 + g], 6 + g, r, above)
+
+    def climb(r):
+        return move(own(r), slot(2, r), 2, r, above)
+
+    @pl.when(y == 0)
+    def _():
+        pl.when(up)(lambda: [climb(r).start() for r in both] and None)
+        across = [move(own(r), slot(1, r), 1, r, partner) for r in both]
+        across += [small(r, g) for g in range(wide) for r in both]
+        for c in across:
+            c.start()
+        side = move(slot(2, 0), slot(3, 0), 3, 0, partner)
+        later = [move(slot(1, r), slot(3, r), 3, r, above, 8) for r in both]
+
+        @pl.when(down)
+        def _():
+            landed(2, 0)
+            side.start()
+            for r in both:
+                landed(1, r)
+                pl.when(up)(later[r].start)
+            landed(2, 1)
+            for g in range(wide):
+                for r in both:
+                    small(r, g).wait_recv()
+            side.wait_send()
+
+            @pl.when(up)
+            def _():
+                for c in later:
+                    c.wait_send()
+
+        @pl.when(down2)
+        def _():
+            for r in both:
+                landed(3, r)
+
+        for c in across:
+            c.wait_send()
+        pl.when(up)(lambda: [climb(r).wait_send() for r in both] and None)
+
+    @pl.when(y == 1)
+    def _():
+        @pl.when(up)
+        def _():
+            for r in both:
+                climb(r).start()
+            for g in range(wide):
+                for r in both:
+                    lift(r, g).start()
+
+        over = [move(slot(2, r), slot(1, r), 1, r, partner) for r in both]
+        on = move(slot(1, 1), slot(3, 1), 3, 1, above)
+        ahead = [small(r, g, staged[r * 2 + g]) for g in range(wide) for r in both]
+
+        @pl.when(down)
+        def _():
+            for r in both:
+                landed(2, r)
+                over[r].start()
+
+        for r in both:
+            landed(1, r)
+        pl.when(up)(on.start)
+
+        @pl.when(down)
+        def _():
+            for g in range(wide):
+                for r in both:
+                    lift(r, g).wait_recv()
+                    small(r, g, staged[r * 2 + g]).start()
+            for r in both:
+                landed(3, r)
+
+        for g in range(wide):
+            for r in both:
+                small(r, g).wait_recv()
+
+        @pl.when(up)
+        def _():
+            on.wait_send()
+            for r in both:
+                climb(r).wait_send()
+                for g in range(wide):
+                    lift(r, g).wait_send()
+
+        @pl.when(down)
+        def _():
+            for c in over + ahead:
+                c.wait_send()
+
+
+def relay_halos(keys, values, n):
+    _, batch, _, cols = keys.shape
+    shapes = tuple(
+        jax.ShapeDtypeStruct((batch, STEPS * d, cols), keys.dtype) for d in DILATIONS
+    )
+    outs = shapes + shapes + shapes[:2] + shapes[:2]
+    return pl.pallas_call(
+        functools.partial(relay_kernel, n),
+        out_shape=outs,
+        in_specs=[pl.BlockSpec(memory_space=pl.ANY)] * 2,
+        out_specs=(pl.BlockSpec(memory_space=pl.ANY),) * len(outs),
+        scratch_shapes=[pltpu.SemaphoreType.DMA((9, 2)), pltpu.SemaphoreType.DMA((9, 2))],
+        compiler_params=pltpu.CompilerParams(collective_id=1, has_side_effects=True),
+    )(keys, values)[: 2 * GROUPS]
+
+
 def exchange_halos(keys, values, n):
+    reaches = [STEPS * d / keys.shape[2] for d in DILATIONS]
+    if n % PAIR == 0 and reaches[0] <= 1 and reaches[1] <= 1 and reaches[2] == 3:
+        return relay_halos(keys, values, n)
     _, batch, rows, cols = keys.shape
     shapes = tuple(
         jax.ShapeDtypeStruct((batch, STEPS * d, cols), keys.dtype) for d in DILATIONS
@@ -293,6 +450,14 @@
     heads = log_ref.shape[1]
     width = cols // heads
     start = place[0] * rows
+
+    def bias(first, count, dilation):
+        lag = lax.broadcasted_iota(jnp.int32, (rows, count), 0) - lax.broadcasted_iota(jnp.int32, (rows, count), 1) - first
+        at = lax.broadcasted_iota(jnp.int32, (rows, count), 1) + (first + start)
+        return (lag >= 0) & (lag <= STEPS * dilation) & ((lag & (dilation - 1)) == 0) & (at >= 0)
+
+    near_ok = [bias(0, rows, d) for d in DILATIONS]
+    far_ok = [bias(-STEPS * d, STEPS * d, d) for d in DILATIONS]
     for h in range(heads):
         lanes = slice(h * width, (h + 1) * width)
         logs, outs = [], []
@@ -300,25 +465,22 @@
             reach = STEPS * dilation
             query = q_ref[g, 0, :, lanes]
 
-            def scored(key, first, count):
+            def scored(key, allowed):
                 score = lax.dot_general(query, key, (((1,), (1,)), ((), ())), preferred_element_type=jnp.float32)
-                score = score * (1.0 / math.sqrt(width))
-                lag = lax.broadcasted_iota(jnp.int32, (rows, count), 0) - lax.broadcasted_iota(jnp.int32, (rows, count), 1) - first
-                at = lax.broadcasted_iota(jnp.int32, (rows, count), 1) + (first + start)
-                allowed = (lag >= 0) & (lag <= reach) & ((lag & (dilation - 1)) == 0) & (at >= 0)
-                return jnp.where(allowed, score, jnp.float32(-1e30))
-
-            near = scored(k_ref[g, 0, :, lanes], 0, rows)
-            far = scored(halos[g][0, :, lanes], -reach, reach)
+                return jnp.where(allowed, score * (1.0 / math.sqrt(width)), jnp.float32(-1e30))
+
+            near = scored(k_ref[g, 0, :, lanes], near_ok[g])
+            far = scored(halos[g][0, :, lanes], far_ok[g])
             peak = jnp.maximum(jnp.max(near, axis=1, keepdims=True), jnp.max(far, axis=1, keepdims=True))
             near, far = jnp.exp(near - peak), jnp.exp(far - peak)
             total = jnp.sum(near, axis=1, keepdims=True) + jnp.sum(far, axis=1, keepdims=True)
             logs.append(peak + jnp.log(total))
+            scale = 1.0 / total
             known = lax.broadcasted_iota(jnp.int32, (reach, width), 0) + (start - reach) >= 0
             old = halos[GROUPS + g][0, :, lanes]
             old = jnp.where(known, old.astype(jnp.float32), 0.0).astype(jnp.bfloat16)
-            mixed = jnp.dot((near / total).astype(jnp.bfloat16), v_ref[g, 0, :, lanes], preferred_element_type=jnp.float32)
-            mixed = mixed + jnp.dot((far / total).astype(jnp.bfloat16), old, preferred_element_type=jnp.float32)
+            mixed = jnp.dot((near * scale).astype(jnp.bfloat16), v_ref[g, 0, :, lanes], preferred_element_type=jnp.float32)
+            mixed = mixed + jnp.dot((far * scale).astype(jnp.bfloat16), old, preferred_element_type=jnp.float32)
             outs.append(mixed.astype(jnp.bfloat16).astype(jnp.float32))
         top = functools.reduce(jnp.maximum, logs)
         shares = [jnp.exp(log - top) for log in logs]

time: 250 us -> 209 us (0.84)
  Pallas kernels: 225 us -> 183 us
    pallas_call x1, Pallas kernels: 87.8 us -> 42.8 us  [relay_halos(): pl.pallas_call(functools.partial(relay_kernel, n), out_shape=outs, in_spe...]
    pallas_call x1, Pallas kernels: 9.18 us -> 12.5 us  [swap_heads(): pl.pallas_call(functools.partial(swap_kernel, m), out_shape=jax.ShapeDtyp...]
where the time goes in v2:
time: 209 us; the launch traced here: 208 us
  Pallas kernels  183 us (88%)
  matrix products  20.1 us (10%)
  other arithmetic  4.53 us (2%)
    pallas_call x1, Pallas kernels, gather_all(): pl.pallas_call(functools.partial(gather_kernel, n, m), out_shape=(jax.Sha...  111 us
    pallas_call x1, Pallas kernels, relay_halos(): pl.pallas_call(functools.partial(relay_kernel, n), out_shape=outs, in_spe...  42.8 us
    pallas_call x1, Pallas kernels, attend(): pl.pallas_call(attend_kernel, grid=(batch,), out_shape=(jax.ShapeDtypeStr...  16.4 us
    dot_general x3, matrix products, project(): jnp.einsum('btd,gdc->gbtc', rows, weight, preferred_element_type=jnp.floa...  15.8 us
    pallas_call x1, Pallas kernels, swap_heads(): pl.pallas_call(functools.partial(swap_kernel, m), out_shape=jax.ShapeDtyp...  12.5 us
    dot_general x1, matrix products, shards(): jnp.einsum('btc,cd->btd', swapped, out_full, preferred_element_type=jnp.f...  4.25 us

profile of v2, /device:TPU:17, one launch (start us, length us, event | category | flops | bytes accessed | tf_op | source)
XLA Modules:
  0.0 208.1 jit_solution(7680120224125943611)
XLA Ops:
  0.6 1.4 fusion.17
  2.0 2.3 %fusion.19.x_ref = bf16[6,32,2048]{2,1,0:T(8,128)(2,1)} fusion(bf16[32,6,2048]{2,0,1:T(8,128)(2,1)} %param.6, f32[2048]{0:T(1024)} %param.7, f32[6,32]{1,0:T(8,128)S(1)} %add_rsqrt_fusion), kind=kLoop, calls=%fused_computation.17 | loop fusion | flops 1572864 | bytes 1581824 | tf_op jit(solution)/shard_map/convert_element_type | solution.py:26
  4.3 111.1 %shard_map.77 = (bf16[6,128,2048]{2,1,0:T(8,128)(2,1)}, bf16[3,2048,256]{2,1,0:T(8,128)(2,1)}, bf16[3,2048,256]{2,1,0:T(8,128)(2,1)}, bf16[3,2048,256]{2,1,0:T(8,128)(2,1)}, bf16[1024,2048]{1,0:T(8,128)(2,1)}) custom-call(bf16[6,32,2048]{2,1,0:T(8,128)(2,1)} %fusion.19.x_ref, bf16[3,256,256]{2,1,0:T(8,128)(2,1)} %q_ref.1, bf16[3,256,256]{2,1,0:T(8,128)(2,1)} %k_ref.1, ...), custom_call_target="tpu_custom_call" | custom-call | tf_op jit(solution)/shard_map/pallas_call | solution.py:197
  115.4 0.0 copy-start.1
  115.4 0.0 copy-start.2
  115.4 6.6 %fusion.35.v_ref = bf16[3,6,128,256]{3,2,1,0:T(8,128)(2,1)} fusion(bf16[6,128,2048]{2,1,0:T(8,128)(2,1)} %get-tuple-element.16, bf16[3,2048,256]{2,1,0:T(8,128)(2,1)} %get-tuple-element.18), kind=kOutput, calls=%fused_computation.21 | convolution fusion | flops 2416508928 | bytes 7471104 | tf_op jit(solution)/shard_map/btd,gdc->gbtc/dot_general | solution.py:558
  122.1 0.0 copy-done.1
  122.1 0.0 copy-done.2
  122.1 3.7 %fusion.40.k_ref = bf16[3,6,128,256]{3,2,1,0:T(8,128)(2,1)} fusion(bf16[6,128,2048]{2,1,0:T(8,128)(2,1)S(1)} %copy-done.1, bf16[3,2048,256]{2,1,0:T(8,128)(2,1)S(1)} %copy-done.2), kind=kOutput, calls=%fused_computation.22 | convolution fusion | flops 2416508928 | bytes 7471104 | tf_op jit(solution)/shard_map/btd,gdc->gbtc/dot_general | solution.py:558
  125.7 42.8 %shard_map.78 = (bf16[6,24,256]{2,1,0:T(8,128)(2,1)}, bf16[6,96,256]{2,1,0:T(8,128)(2,1)}, bf16[6,384,256]{2,1,0:T(8,128)(2,1)}, bf16[6,24,256]{2,1,0:T(8,128)(2...) custom-call(bf16[3,6,128,256]{3,2,1,0:T(8,128)(2,1)} %fusion.40.k_re, ...), custom_call_target="tpu_custom_call" | custom-call | tf_op jit(solution)/shard_map/pallas_call | solution.py:418
  168.5 5.5 %fusion.45.q_ref = bf16[3,6,128,256]{3,2,1,0:T(8,128)(2,1)} fusion(bf16[6,128,2048]{2,1,0:T(8,128)(2,1)S(1)} %copy-done.1, bf16[3,2048,256]{2,1,0:T(8,128)(2,1)} %get-tuple-element.15), kind=kOutput, calls=%fused_computation.23 | convolution fusion | flops 2416508928 | bytes 7471104 | tf_op jit(solution)/shard_map/btd,gdc->gbtc/dot_general | solution.py:558
  174.1 16.4 %shard_map.79 = (bf16[6,128,256]{2,1,0:T(8,128)(2,1)}, f32[6,2,128,1]{3,2,1,0:T(8,128)}) custom-call(s32[1]{0:T(128)} %bitcast.place, bf16[3,6,128,256]{3,2,1,0:T(8,128)(2,1)} %fusion.45.q_ref, bf16[3,6,128,256]{3,2,1,0:T(8,128)(2,1)} %fusion.40.k_ref, bf16[3,6,128,256]{3,2,1,0:T(8,128)(2,1)} %fusion.35.v_ref, ...), custom_call_target="tpu_custom_call" | custom-call | tf_op jit(solution)/shard_map/pallas_call | solution.py:497
  190.5 12.5 %shard_map.80 = bf16[6,32,1024]{2,1,0:T(8,128)(2,1)} custom-call(bf16[6,128,256]{2,1,0:T(8,128)(2,1)} %get-tuple-element.25.c_ref), custom_call_target="tpu_custom_call" | custom-call | tf_op jit(solution)/shard_map/pallas_call | solution.py:542
  203.0 0.0 copy-start
  203.0 4.2 %fusion.14 = bf16[32,6,2048]{2,0,1:T(8,128)(2,1)} fusion(bf16[6,32,1024]{2,1,0:T(8,128)(2,1)} %shard_map.80, bf16[1024,2048]{1,0:T(8,128)(2,1)} %get-tuple-element.26), kind=kOutput, calls=%fused_computation.12 | convolution fusion | flops 805699584 | bytes 5373952 | tf_op jit(solution)/shard_map/btc,cd->btd/dot_general | solution.py:566
  207.3 0.0 copy-done
  207.3 0.9 reduce
  (1 shorter events, 0.0 us)
Async XLA Ops:
  115.4 6.6 %copy-start.1 = (bf16[6,128,2048]{2,1,0:T(8,128)(2,1)S(1)}, bf16[6,128,2048]{2,1,0:T(8,128)(2,1)}, u32[]{:S(2)}) copy-start(bf16[6,128,2048]{2,1,0:T(8,128)(2,1)} %get-tuple-element.16) | copy-start | bytes 9437188
  115.4 6.6 %copy-start.2 = (bf16[3,2048,256]{2,1,0:T(8,128)(2,1)S(1)}, bf16[3,2048,256]{2,1,0:T(8,128)(2,1)}, u32[]{:S(2)}) copy-start(bf16[3,2048,256]{2,1,0:T(8,128)(2,1)} %get-tuple-element.17) | copy-start | bytes 9437188
  203.0 4.3 %copy-start = (f32[6,2,128,1]{3,2,1,0:T(8,128)S(1)}, f32[6,2,128,1]{3,2,1,0:T(8,128)}, u32[]{:S(2)}) copy-start(f32[6,2,128,1]{3,2,1,0:T(8,128)} %get-tuple-element.27) | copy-start | bytes 18436
